TPU v7x, 32 devices: a whole 2x2x4 slice. The times are simulated.
32 devices in a mesh: ep: 8 (over z, core), tp: 4 (over y, x).
Axes of the slice: x: 2, y: 2, z: 4, core: 2. Of those that a mesh axis runs over, the one named last changes fastest.
Arguments:
- mix_in: bfloat16 [2048, 2048], P('ep'), may hold values from -6 to 6
- mix_gain: float32 [2048], replicated, may hold values from 0.1 to 1.9
- w_in_x: bfloat16 [2048, 2048], P(None, 'tp'), may hold values from -0.125 to 0.125
- w_in_y: bfloat16 [2048, 2048], P(None, 'tp'), may hold values from -0.125 to 0.125
- conv_taps: float32 [4, 2048], P(None, 'tp'), may hold values from -3 to 3
- recur_gate_w: bfloat16 [16, 128, 128], P('tp'), may hold values from -0.5 to 0.5
- input_gate_w: bfloat16 [16, 128, 128], P('tp'), may hold values from -0.5 to 0.5
- decay_logit: float32 [2048], P('tp'), may hold values from 4 to 20
- decay_shift: float32 [2048, 2048], P('ep', 'tp'), may hold values from -2.2 to 0
- moe_in: bfloat16 [2048, 2048], P('ep'), may hold values from -6 to 6
- moe_gain: float32 [2048], replicated, may hold values from 0.1 to 1.9
- routes: int32 [2048, 2], P('ep'), may hold values from 0 to 7, all different within a row; in each aligned block of 256 rows (0 to 255, 256 to 511, ...) at most 128 rows name the same one
- route_weight: float32 [2048, 2], P('ep'), may hold values from 0.1 to 1
- expert_gate: bfloat16 [8, 2048, 2048], P('ep', None, 'tp'), may hold values from -0.125 to 0.125
- expert_up: bfloat16 [8, 2048, 2048], P('ep', None, 'tp'), may hold values from -0.125 to 0.125
- expert_down: bfloat16 [8, 2048, 2048], P('ep', None, 'tp'), may hold values from -0.125 to 0.125
Outputs:
- mixer_out: bfloat16 [2048, 2048], P('ep', 'tp')
- moe_out: bfloat16 [2048, 2048], P('ep', 'tp')
Inputs may be any that keep to these rules, and one draw needn't show every extreme that they name: `routes`: each row names 2 different experts. Among the rows of one index of ep no expert is named more than 128 times, a bound that some block reaches.
All inputs are finite; a program needn't handle non-finite values.
Results may differ from a plain program's by a relative error of at most 0.0095.
Values may be sent and summed in bfloat16 or wider, within the bound.
A program may use at most 64 MiB of HBM per device.

v0:
```python
import jax
import jax.numpy as jnp
from jax import lax
from jax.sharding import PartitionSpec as P

epsilon = 1e-06
lru_scale = 8.0


def from_behind(value, axis, by):
    count = lax.axis_size(axis)
    pairs = [(i, i + by) for i in range(count) if 0 <= i + by < count]
    return lax.ppermute(value, axis, pairs)


def entering(value, axis, combine, identity):
    count, index = (lax.axis_size(axis), lax.axis_index(axis))
    everything = jax.tree.map(lambda part: lax.all_gather(part, axis), value)
    start = jax.tree.map(
        lambda part, zero: jnp.broadcast_to(jnp.asarray(zero, part.dtype), part.shape),
        value,
        identity,
    )

    def hop(k, before):
        reached = k < index
        new = combine(before, jax.tree.map(lambda part: part[k], everything))
        return jax.tree.map(lambda a, b: jnp.where(reached, a, b), new, before)

    return lax.fori_loop(0, count, hop, start)


def norm_rows(rows, gain):
    widened = rows.astype(jnp.float32)
    scaled = widened * lax.rsqrt(jnp.mean(widened * widened, axis=-1, keepdims=True) + epsilon)
    return (scaled * gain[None, :]).astype(jnp.bfloat16)


def link(earlier, later):
    return (earlier[0] * later[0], later[0] * earlier[1] + later[1])


def local(
    mix_in,
    mix_gain,
    w_in_x,
    w_in_y,
    conv_taps,
    recur_gate_w,
    input_gate_w,
    decay_logit,
    decay_shift,
    moe_in,
    moe_gain,
    routes,
    route_weight,
    expert_gate,
    expert_up,
    expert_down,
):
    row_count = mix_in.shape[0]
    width_dev = w_in_x.shape[1]
    heads_dev = recur_gate_w.shape[0]
    block_size = recur_gate_w.shape[1]
    tap_count = conv_taps.shape[0]
    mixer_rows = norm_rows(mix_in, mix_gain)
    x_branch = jnp.dot(mixer_rows, w_in_x, preferred_element_type=jnp.float32).astype(jnp.bfloat16)
    y_branch = jnp.dot(mixer_rows, w_in_y, preferred_element_type=jnp.float32).astype(jnp.bfloat16)
    previous = from_behind(x_branch[row_count - (tap_count - 1) :], "ep", 1)
    padded = jnp.concatenate([previous, x_branch], axis=0)
    conv_sum = jnp.zeros((row_count, width_dev), jnp.float32)
    for tap_index in range(tap_count):
        conv_sum = conv_sum + conv_taps[tap_index][None, :] * padded[
            tap_index : tap_index + row_count
        ].astype(jnp.float32)
    x_conv = conv_sum.astype(jnp.bfloat16)
    heads_in = x_conv.reshape(row_count, heads_dev, block_size)
    gate_a = jnp.einsum(
        "thi,hij->thj", heads_in, recur_gate_w, preferred_element_type=jnp.float32
    ).reshape(row_count, width_dev)
    gate_x = jnp.einsum(
        "thi,hij->thj", heads_in, input_gate_w, preferred_element_type=jnp.float32
    ).reshape(row_count, width_dev)
    log_decay = (
        -lru_scale * jax.nn.sigmoid(gate_a) * jax.nn.softplus(-decay_logit)[None, :] + decay_shift
    )
    lru_drive = (
        jnp.sqrt(-jnp.expm1(2.0 * log_decay)) * jax.nn.sigmoid(gate_x) * x_conv.astype(jnp.float32)
    )
    through, local_state = lax.associative_scan(link, (jnp.exp(log_decay), lru_drive), axis=0)
    identity = (jnp.ones((width_dev,), jnp.float32), jnp.zeros((width_dev,), jnp.float32))
    carried = entering((through[row_count - 1], local_state[row_count - 1]), "ep", link, identity)
    lru_state = local_state + through * carried[1][None, :]
    mixer_out = (lru_state * jax.nn.gelu(y_branch.astype(jnp.float32))).astype(jnp.bfloat16)
    moe_rows = norm_rows(moe_in, moe_gain)
    token_count = moe_rows.shape[0]
    feature_count = moe_rows.shape[1]
    choose_count = routes.shape[1]
    expert_count = lax.axis_size("ep")
    capacity = 2 * token_count * choose_count // expert_count
    slot_total = expert_count * capacity
    expert_ids = routes.reshape(-1)
    onehot = (expert_ids[:, None] == jnp.arange(expert_count, dtype=jnp.int32)[None, :]).astype(
        jnp.int32
    )
    slot_rank = jnp.sum(jnp.cumsum(onehot, axis=0) * onehot, axis=1) - 1
    slot_index = expert_ids * capacity + slot_rank
    token_index = jnp.repeat(jnp.arange(token_count, dtype=jnp.int32), choose_count)
    slot_owner = jnp.full((slot_total,), token_count, jnp.int32).at[slot_index].set(token_index)
    padded_rows = jnp.concatenate([moe_rows, jnp.zeros((1, feature_count), jnp.bfloat16)], axis=0)
    outgoing = padded_rows[slot_owner].reshape(expert_count, capacity, feature_count)
    column_width = feature_count // lax.axis_size("tp")
    own_columns = lax.dynamic_slice_in_dim(
        outgoing, lax.axis_index("tp") * column_width, column_width, 2
    )
    incoming = lax.all_to_all(own_columns, "ep", split_axis=0, concat_axis=0, tiled=True)
    piece = lax.all_gather(incoming, "tp", axis=2, tiled=True)
    flat_rows = piece.reshape(slot_total, piece.shape[2])
    gate_rows = expert_gate[0]
    up_rows = expert_up[0]
    gate_proj = jnp.dot(flat_rows, gate_rows, preferred_element_type=jnp.float32)
    up_proj = jnp.dot(flat_rows, up_rows, preferred_element_type=jnp.float32)
    hidden = (jax.nn.silu(gate_proj) * up_proj).astype(jnp.bfloat16)
    down_rows = expert_down[0]
    columns = jnp.dot(
        lax.all_gather(hidden, "tp", axis=1, tiled=True),
        down_rows,
        preferred_element_type=jnp.float32,
    )
    results = columns.astype(jnp.bfloat16).reshape(expert_count, capacity, expert_down.shape[2])
    returned = lax.all_to_all(results, "ep", split_axis=0, concat_axis=0, tiled=True).reshape(
        slot_total, expert_down.shape[2]
    )
    picked = (
        returned[slot_index]
        .astype(jnp.float32)
        .reshape(token_count, choose_count, expert_down.shape[2])
    )
    route_share = route_weight / jnp.sum(route_weight, axis=1, keepdims=True)
    moe_out = jnp.sum(route_share[:, :, None] * picked, axis=1).astype(jnp.bfloat16)
    return (mixer_out, moe_out)


def solution(mesh):
    placed = (
        P("ep", None),
        P(),
        P(None, "tp"),
        P(None, "tp"),
        P(None, "tp"),
        P("tp", None, None),
        P("tp", None, None),
        P("tp"),
        P("ep", "tp"),
        P("ep", None),
        P(),
        P("ep", None),
        P("ep", None),
        P("ep", None, "tp"),
        P("ep", None, "tp"),
        P("ep", None, "tp"),
    )
    return jax.shard_map(
        local, mesh=mesh, in_specs=placed, out_specs=(P("ep", "tp"), P("ep", "tp")), check_vma=False
    )
```

profile of v0, /device:TPU:1, one launch (start us, length us, event | category | flops | bytes accessed | tf_op | source)
XLA Modules:
  0.0 282.8 jit_solution(14209495019624665678)
XLA Ops:
  11.2 2.4 scatter_custom_fusion
  15.6 6.0 %gather_fusion = bf16[1024,2048]{1,0:T(8,128)(2,1)} fusion(bf16[257,2048]{1,0:T(8,128)(2,1)S(1)} %concatenate.63, s32[1024]{0:T(1024)S(1)} %fusion.50), kind=kCustom, calls=%fused_computation | custom fusion | bytes 8392704 | tf_op jit(solution)/shard_map/gather | solution.py:111
  22.9 31.9 %all_to_all.10 = bf16[8,128,512]{2,1,0:T(8,128)(2,1)} all-to-all(bf16[8,128,512]{2,1,0:T(8,128)(2,1)S(1)} %constant_dynamic-slice_fusion.2), channel_id=1, replica_groups=mesh['ep'=8,'tp'=4] {'ep'}, dimensions={0} | all-to-all | bytes 2097152 | tf_op jit(solution)/shard_map/all_to_all | solution.py:116
  55.8 2.4 convolution_convert_fusion.1
  58.9 2.5 collective-permute-start
  62.9 1.7 add_convert_fusion
  64.6 42.0 %all-gather.5.cloned.1.call-done = bf16[8,128,2048]{2,1,0:T(8,128)(2,1)} async-done(((bf16[8,128,512]{2,1,0:T(8,128)(2,1)}), bf16[8,128,2048]{2,1,0:T(8,128)(2,1)}) %all-gather.5.cloned.1.call-update) | async-done | bytes 4194320 | tf_op jit(solution)/shard_map/all_gather | solution.py:117
  106.6 4.7 %fusion.8 = f32[1024,512]{1,0:T(8,128)S(1)} fusion(bf16[1024,2048]{1,0:T(8,128)(2,1)} %bitcast.86, bf16[1,2048,512]{2,1,0:T(8,128)(2,1)S(1)} %copy-done), kind=kOutput, calls=%fused_computation.18 | convolution fusion | flops 2147483648 | bytes 8388608 | tf_op jit(solution)/shard_map/dot_general | solution.py:122
  111.3 3.7 %multiply_convert_fusion = bf16[1024,512]{1,0:T(8,128)(2,1)} fusion(f32[1024,512]{1,0:T(8,128)S(1)} %fusion.8, bf16[1024,2048]{1,0:T(8,128)(2,1)S(1)} %bitcast.87, bf16[1,2048,512]{2,1,0:T(8,128)(2,1)S(1)} %copy-done.24), kind=kOutput, calls=%fused_computation.22 | convolution fusion | flops 2150629376 | bytes 9437184 | tf_op jit(solution)/shard_map/dot_general | solution.py:121
  117.7 1.8 convert_multiply_fusion.4
  125.0 2.0 multiply_add_fusion.1
  131.6 1.8 multiply_add_fusion.2
  199.0 1.7 pad.114
  200.8 1.9 fusion.39
  203.6 13.5 %all-gather.1 = f32[8,1,512]{2,1,0:T(1,128)S(1)} all-gather(f32[1,1,512]{2,1,0:T(1,128)S(1)} %add_bitcast_fusion), channel_id=1, replica_groups=mesh['ep'=8,'tp'=4] {'ep'}, dimensions={0}, use_global_device_ids=true | all-gather | bytes 18432 | tf_op jit(solution)/shard_map/all_gather | solution.py:18
  217.1 1.7 pad.130
  221.2 12.8 %all-gather = f32[8,1,512]{2,1,0:T(1,128)S(1)} all-gather(f32[1,1,512]{2,1,0:T(1,128)S(1)} %add_bitcast_fusion.1), channel_id=1, replica_groups=mesh['ep'=8,'tp'=4] {'ep'}, dimensions={0}, use_global_device_ids=true | all-gather | bytes 18432 | tf_op jit(solution)/shard_map/all_gather | solution.py:18
  233.9 6.2 %fusion.14 = bf16[1024,512]{1,0:T(8,128)(2,1)} fusion(bf16[1024,2048]{1,0:T(8,128)(2,1)} %all-gather.7.cloned.1.call-done, bf16[1,2048,512]{2,1,0:T(8,128)(2,1)} %param.33), kind=kOutput, calls=%fused_computation.23 | convolution fusion | flops 2148007936 | bytes 7340032 | tf_op jit(solution)/shard_map/dot_general | solution.py:125
  240.2 3.9 %all-to-all-start.1 = ((bf16[8,128,512]{2,1,0:T(8,128)(2,1)}), bf16[8,128,512]{2,1,0:T(8,128)(2,1)S(1)}, u32[]{:S(2)}, u32[]{:S(2)}) async-start(bf16[8,128,512]{2,1,0:T(8,128)(2,1)} %bitcast.72), calls=%async_computation.1 | async-start | bytes 2097152 | tf_op jit(solution)/shard_map/all_to_all | solution.py:131
  244.5 4.1 %fusion.32 = bf16[256,512]{1,0:T(8,128)(2,1)} fusion(bf16[2048,512]{1,0:T(8,128)(2,1)} %param.21, f32[256,512]{1,0:T(8,128)} %pad.129, f32[256,512]{1,0:T(8,128)} %pad.130, f32[256,512]{1,0:T(8,128)} %copy-done.4, f32[256,512]{1,0:T(8,128)} %pad.114, bf16[256,2048]{1,0:T(8,128)(2,1)} %param.18, f32[2048]{0:T(1024)S(1)} %copy-done.28, ...), kind=kOutput, calls=%fused_computation.45 | convolution fusion | flops 541065216 | bytes 5516288 | tf_op jit(solution)/shard_map/dot_general | solution.py:68
  248.6 20.9 %all-to-all-done.1 = bf16[8,128,512]{2,1,0:T(8,128)(2,1)S(1)} async-done(((bf16[8,128,512]{2,1,0:T(8,128)(2,1)}), bf16[8,128,512]{2,1,0:T(8,128)(2,1)S(1)}, u32[]{:S(2)}, u32[]{:S(2)}) %all-to-all-start.1) | async-done | bytes 1048608 | tf_op jit(solution)/shard_map/all_to_all | solution.py:131
  269.6 2.6 gather_fusion.1
  272.2 1.7 reshape.120
  273.9 2.1 multiply_reduce_fusion
  (237 shorter events, 92.4 us)
Async XLA Ops:
  7.2 99.4 %copy-start = (bf16[1,2048,512]{2,1,0:T(8,128)(2,1)S(1)}, bf16[1,2048,512]{2,1,0:T(8,128)(2,1)}, u32[]{:S(2)}) copy-start(bf16[1,2048,512]{2,1,0:T(8,128)(2,1)} %param.32) | copy-start | bytes 6291460
  7.2 8.0 %copy-start.1 = (bf16[256,2048]{1,0:T(8,128)(2,1)S(1)}, bf16[256,2048]{1,0:T(8,128)(2,1)}, u32[]{:S(2)}) copy-start(bf16[256,2048]{1,0:T(8,128)(2,1)} %param.27) | copy-start | bytes 3145732
  7.2 8.0 %copy-start.12 = (f32[2048]{0:T(1024)S(1)}, f32[2048]{0:T(1024)}, u32[]{:S(2)}) copy-start(f32[2048]{0:T(1024)} %param.28) | copy-start | bytes 24580
  7.2 99.4 %all-gather.5.cloned.1.call-start = ((), (), s32[]{:S(2)}) async-start(), calls=%async_computation.2 | async-start | bytes 5242880 | tf_op jit(solution)/shard_map/all_gather | solution.py:117
  22.9 32.0 %copy-start.2 = (bf16[256,2048]{1,0:T(8,128)(2,1)S(1)}, bf16[256,2048]{1,0:T(8,128)(2,1)}, u32[]{:S(2)}) copy-start(bf16[256,2048]{1,0:T(8,128)(2,1)} %param.18) | copy-start | bytes 3145732
  22.9 32.9 %copy-start.27 = (f32[2048]{0:T(1024)S(1)}, f32[2048]{0:T(1024)}, u32[]{:S(2)}) copy-start(f32[2048]{0:T(1024)} %param.19) | copy-start | bytes 24580
  54.9 179.1 %all-gather.7.cloned.1.call-start = ((), (), s32[]{:S(2)}) async-start(), calls=%async_computation.3 | async-start | bytes 5242880 | tf_op jit(solution)/shard_map/all_gather | solution.py:126
  55.8 5.6 %copy-start.18 = (f32[256,2]{0,1:T(2,128)S(1)}, f32[256,2]{0,1:T(2,128)}, u32[]{:S(2)}) copy-start(f32[256,2]{0,1:T(2,128)} %param.30) | copy-start | bytes 6148
  55.8 5.6 %copy-start.20 = (f32[512]{0:T(512)S(1)}, f32[512]{0:T(512)}, u32[]{:S(2)}) copy-start(f32[512]{0:T(512)} %param.25) | copy-start | bytes 6148
  55.8 5.6 %copy-start.19 = (f32[4,512]{1,0:T(4,128)S(1)}, f32[4,512]{1,0:T(4,128)}, u32[]{:S(2)}) copy-start(f32[4,512]{1,0:T(4,128)} %param.22) | copy-start | bytes 24580
  58.9 4.0 %collective-permute-start = (bf16[3,512]{1,0:T(4,128)(2,1)S(1)}, bf16[3,512]{1,0:T(4,128)(2,1)S(1)}, u32[]{:S(2)}, u32[]{:S(2)}) collective-permute-start(bf16[3,512]{1,0:T(4,128)(2,1)S(1)} %slice.356), channel_id=1, source_target_pairs={{0,4},{4,8},{8,12},{12,16},{16,20},{20,24},{24,28},{1,5},{5,9},{9,... | collective-permute-start | bytes 9224 | tf_op jit(solution)/shard_map/ppermute | solution.py:13
  106.6 4.7 %copy-start.23 = (bf16[8,128,2048]{2,1,0:T(8,128)(2,1)S(1)}, bf16[8,128,2048]{2,1,0:T(8,128)(2,1)}, u32[]{:S(2)}) copy-start(bf16[8,128,2048]{2,1,0:T(8,128)(2,1)} %all-gather.5.cloned.1.call-done) | copy-start | bytes 12582916
  106.6 4.7 %copy-start.24 = (bf16[1,2048,512]{2,1,0:T(8,128)(2,1)S(1)}, bf16[1,2048,512]{2,1,0:T(8,128)(2,1)}, u32[]{:S(2)}) copy-start(bf16[1,2048,512]{2,1,0:T(8,128)(2,1)} %param.31) | copy-start | bytes 6291460
  185.6 12.3 %copy-start.8 = (f32[31,512]{1,0:T(8,128)S(1)}, f32[31,512]{1,0:T(8,128)}, u32[]{:S(2)}) copy-start(f32[31,512]{1,0:T(8,128)} %slice.287) | copy-start | bytes 190468
  185.6 12.3 %copy-start.9 = (f32[31,512]{1,0:T(8,128)S(1)}, f32[31,512]{1,0:T(8,128)}, u32[]{:S(2)}) copy-start(f32[31,512]{1,0:T(8,128)} %slice.328) | copy-start | bytes 190468
  188.9 9.0 %copy-start.17 = (f32[1,512]{1,0:T(1,128)S(1)}, f32[1,512]{1,0:T(1,128)}, u32[]{:S(2)}) copy-start(f32[1,512]{1,0:T(1,128)} %slice.389) | copy-start | bytes 6148
  193.3 5.4 %copy-start.6 = (f32[63,512]{1,0:T(8,128)S(1)}, f32[63,512]{1,0:T(8,128)}, u32[]{:S(2)}) copy-start(f32[63,512]{1,0:T(8,128)} %slice.330) | copy-start | bytes 387076
  200.8 17.9 %copy-start.13 = (f32[1,512]{1,0:T(1,128)S(1)}, f32[1,512]{1,0:T(1,128)}, u32[]{:S(2)}) copy-start(f32[1,512]{1,0:T(1,128)} %slice.387) | copy-start | bytes 6148
  202.7 16.0 %copy-start.3 = (f32[127,512]{1,0:T(8,128)S(1)}, f32[127,512]{1,0:T(8,128)}, u32[]{:S(2)}) copy-start(f32[127,512]{1,0:T(8,128)} %get-tuple-element.130) | copy-start | bytes 780292
  202.8 37.3 %copy-start.4 = (f32[256,512]{1,0:T(8,128)}, f32[256,512]{1,0:T(8,128)S(1)}, u32[]{:S(2)}) copy-start(f32[256,512]{1,0:T(8,128)S(1)} %pad.113) | copy-start | bytes 1572868
  240.1 4.3 %copy-start.22 = (f32[256]{0:T(256)S(1)}, f32[256]{0:T(256)}, u32[]{:S(2)}) copy-start(f32[256]{0:T(256)} %copy-done.21) | copy-start | bytes 3076
  240.1 4.4 %copy-start.28 = (f32[2048]{0:T(1024)S(1)}, f32[2048]{0:T(1024)}, u32[]{:S(2)}) copy-start(f32[2048]{0:T(1024)} %param.19) | copy-start | bytes 24580
  240.2 29.4 %all-to-all-start.1 = ((bf16[8,128,512]{2,1,0:T(8,128)(2,1)}), bf16[8,128,512]{2,1,0:T(8,128)(2,1)S(1)}, u32[]{:S(2)}, u32[]{:S(2)}) async-start(bf16[8,128,512]{2,1,0:T(8,128)(2,1)} %bitcast.72), calls=%async_computation.1 | async-start | bytes 2097152 | tf_op jit(solution)/shard_map/all_to_all | solution.py:131
  244.5 25.0 %copy-start.11 = (s32[1024]{0:T(1024)S(1)}, s32[1024]{0:T(1024)}, u32[]{:S(2)}) copy-start(s32[1024]{0:T(1024)} %pad_clamp_fusion) | copy-start | bytes 12292
  (9 other events, 20.4 us)
Sparse Core Ops, SparseCore 0:
  55.0 51.5 all-gather.4
  115.1 52.4 all-gather.6
where the time goes:
time: 286 us; the launch traced here: 283 us
  local copies, waits for them, and re-layouts  86.2 us (30%)
  waiting for transfers between devices  63 us (22%)
  blocking collectives  58.2 us (20%)
  other arithmetic  32.3 us (11%)
  matrix products  21.7 us (8%)
  between operations  14.8 us (5%)
  starting transfers between devices  6.42 us (2%)
    slice x52, local copies, waits for them, and re-layouts, local(): lax.associative_scan(link, (jnp.exp(log_decay), lru_drive), axis=0)  60.4 us
    all_gather x1, waiting for transfers between devices, local(): piece = lax.all_gather(incoming, 'tp', axis=2, tiled=True)  42 us
    all_to_all x1, blocking collectives, local(): lax.all_to_all(own_columns, 'ep', split_axis=0, concat_axis=0, tiled=True)  31.9 us
    all_gather x2, blocking collectives, entering(): everything = jax.tree.map(lambda part: lax.all_gather(part, axis), value)  26.2 us
    all_to_all x1, waiting for transfers between devices, local(): lax.all_to_all(results, 'ep', split_axis=0, concat_axis=0, tiled=True)  20.9 us
    add x13, other arithmetic, link(): return (earlier[0] * later[0], later[0] * earlier[1] + later[1])  14.6 us
    dot_general x1, matrix products, local(): jnp.dot(lax.all_gather(hidden, 'tp', axis=1, tiled=True), down_rows, pref...  6.22 us
    gather x1, local copies, waits for them, and re-layouts, local(): padded_rows[slot_owner].reshape(expert_count, capacity, feature_count)  5.98 us
  transfers between devices with their start and end apart: 4, of which 2 were waited for; matrix products, arithmetic and copies ran while one was open for 36% of the time, Pallas kernels for 0%

commit v1 on v0

--- a/solution.py
+++ b/solution.py
@@ -1,10 +1,430 @@
+import functools
+
 import jax
 import jax.numpy as jnp
 from jax import lax
+from jax.experimental import pallas as pl
+from jax.experimental.pallas import tpu as pltpu
 from jax.sharding import PartitionSpec as P
 
 epsilon = 1e-06
 lru_scale = 8.0
+MESH = pl.DeviceIdType.MESH
+F32 = jnp.float32
+BF16 = jnp.bfloat16
+
+
+def near_first(count):
+    return [sorted(range(count), key=lambda q: (abs(q - z), -q)) for z in range(count)]
+
+
+def moe_kernel(
+    cap,
+    moe_hbm,
+    gain_ref,
+    rt_row,
+    rt_col,
+    rw_col,
+    gate_hbm,
+    up_hbm,
+    down_hbm,
+    out_ref,
+    tok,
+    hid,
+    xs,
+    res,
+    ret,
+    routes_all,
+    gw,
+    uw,
+    dw,
+    load_sem,
+    rt_sem,
+    z_send,
+    z_recv,
+    t_sem,
+    sib_sem,
+    own_sem,
+    h_sem,
+    ret_sem,
+):
+    n_ep = lax.axis_size("ep")
+    nz = n_ep // 2
+    ep = lax.axis_index("ep")
+    t = lax.axis_index("tp")
+    z, c = ep // 2, ep % 2
+    y, x = t // 2, t % 2
+    xp, yp, dg = y * 2 + (1 - x), (1 - y) * 2 + x, 3 - t
+    rows, share = tok.shape[3], tok.shape[4]
+    half = rows // 2
+    pair = 2 * cap
+    pair_half = pair // 2
+    sibling = {"ep": z * 2 + (1 - c)}
+    table = near_first(nz)
+
+    def block_at(s):
+        q = jnp.int32(0)
+        for zz in range(nz):
+            for ss in range(nz):
+                q = jnp.where((z == zz) & (s == ss), table[zz][ss], q)
+        return q
+
+    def remote(src, dst, send, recv, where):
+        return pltpu.make_async_remote_copy(
+            src_ref=src,
+            dst_ref=dst,
+            send_sem=send,
+            recv_sem=recv,
+            device_id=where,
+            device_id_type=MESH,
+        )
+
+    loads = [
+        pltpu.make_async_copy(
+            moe_hbm.at[:, pl.ds(k * share, share)], tok.at[c, z, k], load_sem.at[k]
+        )
+        for k in range(4)
+    ] + [
+        pltpu.make_async_copy(gate_hbm.at[0], gw, load_sem.at[4]),
+        pltpu.make_async_copy(up_hbm.at[0], uw, load_sem.at[5]),
+        pltpu.make_async_copy(down_hbm.at[0], dw, load_sem.at[6]),
+    ]
+    for copy in loads:
+        copy.start()
+
+    barrier = pltpu.get_barrier_semaphore()
+    for by in range(1, n_ep):
+        pl.semaphore_signal(
+            barrier, inc=1, device_id={"ep": (ep + by) % n_ep}, device_id_type=MESH
+        )
+    for peer in (xp, yp):
+        pl.semaphore_signal(barrier, inc=1, device_id={"tp": peer}, device_id_type=MESH)
+    pl.semaphore_wait(barrier, n_ep + 1)
+
+    def route_copy(by):
+        return remote(
+            rt_row,
+            routes_all.at[ep],
+            rt_sem.at[0, by],
+            rt_sem.at[1, ep],
+            {"ep": (ep + by) % n_ep},
+        )
+
+    for by in range(1, n_ep):
+        route_copy(by).start()
+    routes_all[ep] = rt_row[...]
+
+    def z_copy(q, up):
+        return remote(
+            tok.at[c, q, t],
+            tok.at[c, q, t],
+            z_send.at[up, q],
+            z_recv.at[q],
+            {"ep": ep + (2 if up else -2)},
+        )
+
+    def t_copy(q, kind):
+        if kind == 0:
+            part, where = tok.at[c, q, t], {"tp": xp}
+        elif kind == 1:
+            part, where = tok.at[c, q, t], {"tp": yp}
+        elif kind == 2:
+            part, where = tok.at[c, q, yp, pl.ds(half, half)], {"tp": xp}
+        else:
+            part, where = tok.at[c, q, xp, pl.ds(0, half)], {"tp": yp}
+        return remote(part, part, t_sem.at[0, kind, q], t_sem.at[1, kind, q], where)
+
+    def sib_copy(q, k):
+        part = tok.at[c, q, k]
+        return remote(part, part, sib_sem.at[0, k, q], sib_sem.at[1, k, q], sibling)
+
+    def own_copy():
+        part = tok.at[c, z]
+        return remote(part, part, own_sem.at[0], own_sem.at[1], sibling)
+
+    def h_copy(q, kind):
+        if kind == 0:
+            part, where = hid.at[q, t], {"tp": xp}
+        elif kind == 1:
+            part, where = hid.at[q, t], {"tp": yp}
+        elif kind == 2:
+            part, where = hid.at[q, yp, pl.ds(pair_half, pair_half)], {"tp": xp}
+        else:
+            part, where = hid.at[q, xp, pl.ds(0, pair_half)], {"tp": yp}
+        return remote(part, part, h_sem.at[0, kind, q], h_sem.at[1, kind, q], where)
+
+    def ret_copy(q, cc):
+        part = res.at[q * 2 + cc]
+        return remote(
+            part, ret.at[ep], ret_sem.at[0, q * 2 + cc], ret_sem.at[1, ep], {"ep": q * 2 + cc}
+        )
+
+    def spread(q):
+        t_copy(q, 0).start()
+        t_copy(q, 1).start()
+
+        @pl.when((q < z) & (z + 1 < nz))
+        def _():
+            z_copy(q, 1).start()
+
+        @pl.when((q > z) & (z > 0))
+        def _():
+            z_copy(q, 0).start()
+
+        sib_copy(q, t).start()
+
+    def ranks_row(block):
+        named = routes_all[block]
+        mask = jnp.where((named[0:1] == ep) | (named[1:2] == ep), 1.0, 0.0)
+        before = jnp.where(
+            lax.broadcasted_iota(jnp.int32, (rows, rows), 0)
+            < lax.broadcasted_iota(jnp.int32, (rows, rows), 1),
+            1.0,
+            0.0,
+        ).astype(BF16)
+        rank = jnp.dot(
+            jnp.broadcast_to(mask, (8, rows)).astype(BF16), before, preferred_element_type=F32
+        )[0:1]
+        key = jnp.where(mask > 0.5, rank, -1.0)
+        seat = lax.broadcasted_iota(jnp.int32, (cap, rows), 0).astype(F32)
+        return jnp.where(seat == key, 1.0, 0.0).astype(BF16)
+
+    def expert_in(q):
+        for cc in range(2):
+            pick = ranks_row(q * 2 + cc)
+            parts = [
+                jnp.dot(pick, tok[cc, q, k], preferred_element_type=F32) for k in range(4)
+            ]
+            square = sum(jnp.sum(part * part, axis=-1, keepdims=True) for part in parts)
+            scale = lax.rsqrt(square * (1.0 / (4 * share)) + epsilon)
+            for k in range(4):
+                xs[pl.ds(cc * cap, cap), pl.ds(k * share, share)] = (
+                    parts[k] * scale * gain_ref[:, pl.ds(k * share, share)]
+                ).astype(BF16)
+
+        tile = 256
+
+        @pl.loop(0, gw.shape[1] // tile)
+        def _(j):
+            cols = pl.ds(pl.multiple_of(j * tile, tile), tile)
+            g = jnp.dot(xs[...], gw[:, cols], preferred_element_type=F32)
+            u = jnp.dot(xs[...], uw[:, cols], preferred_element_type=F32)
+            hid[q, t, :, cols] = (jax.nn.silu(g) * u).astype(BF16)
+
+        h_copy(q, 0).start()
+        h_copy(q, 1).start()
+
+    def expert_out(q):
+        tile = 256
+        span = hid.shape[3]
+
+        @pl.loop(0, dw.shape[1] // tile)
+        def _(j):
+            cols = pl.ds(pl.multiple_of(j * tile, tile), tile)
+            total = jnp.zeros((pair, tile), F32)
+            for k in range(4):
+                total = total + jnp.dot(
+                    hid[q, k], dw[pl.ds(k * span, span), cols], preferred_element_type=F32
+                )
+            out = total.astype(BF16)
+            res[q * 2, :, cols] = out[:cap]
+            res[q * 2 + 1, :, cols] = out[cap:]
+
+        for cc in range(2):
+            mine = (q == z) & (c == cc)
+
+            @pl.when(jnp.logical_not(mine))
+            def _():
+                ret_copy(q, cc).start()
+
+            @pl.when(mine)
+            def _():
+                ret[ep] = res[q * 2 + cc]
+
+    for k in range(4):
+        loads[k].wait()
+
+    @pl.when(z + 1 < nz)
+    def _():
+        z_copy(z, 1).start()
+
+    @pl.when(z > 0)
+    def _():
+        z_copy(z, 0).start()
+
+    own_copy().start()
+    for k in range(4, 7):
+        loads[k].wait()
+    for by in range(1, n_ep):
+        other = (ep + by) % n_ep
+        remote(
+            rt_row, routes_all.at[other], rt_sem.at[0, 0], rt_sem.at[1, other], {"ep": other}
+        ).wait_recv()
+    remote(
+        tok.at[1 - c, z], tok.at[1 - c, z], own_sem.at[0], own_sem.at[1], sibling
+    ).wait_recv()
+    expert_in(z)
+    first = block_at(1)
+    z_copy(first, 1).wait_recv()
+    spread(first)
+
+    def step(s, carry):
+        q = block_at(s)
+        nxt = block_at(s + 1)
+        far = block_at(s + 2)
+        h_copy(q, 0).wait_recv()
+        h_copy(q, 3).start()
+        h_copy(q, 1).wait_recv()
+        h_copy(q, 2).start()
+
+        @pl.when(s + 1 < nz)
+        def _():
+            t_copy(nxt, 0).wait_recv()
+            t_copy(nxt, 3).start()
+            sib_copy(nxt, xp).start()
+            t_copy(nxt, 1).wait_recv()
+            t_copy(nxt, 2).start()
+            sib_copy(nxt, yp).start()
+
+            @pl.when(s + 2 < nz)
+            def _():
+                z_copy(far, 1).wait_recv()
+                spread(far)
+
+            t_copy(nxt, 2).wait_recv()
+            t_copy(nxt, 3).wait_recv()
+            sib_copy(nxt, dg).start()
+            for k in range(4):
+                sib_copy(nxt, k).wait_recv()
+            expert_in(nxt)
+
+        h_copy(q, 2).wait_recv()
+        h_copy(q, 3).wait_recv()
+        expert_out(q)
+        return carry
+
+    lax.fori_loop(0, nz, step, 0)
+
+    one, two = rt_col[:, 0:1], rt_col[:, 1:2]
+    lane = lax.broadcasted_iota(jnp.int32, (rows, 128), 1)
+    mask = jnp.where((one == lane) | (two == lane), 1.0, 0.0)
+    before = jnp.where(
+        lax.broadcasted_iota(jnp.int32, (rows, rows), 1)
+        < lax.broadcasted_iota(jnp.int32, (rows, rows), 0),
+        1.0,
+        0.0,
+    ).astype(BF16)
+    rank = jnp.dot(before, mask.astype(BF16), preferred_element_type=F32)
+    key = jnp.where(mask > 0.5, rank, -1.0)
+    total_weight = rw_col[:, 0:1] + rw_col[:, 1:2]
+    part_one = rw_col[:, 0:1] / total_weight
+    part_two = rw_col[:, 1:2] / total_weight
+    seat = lax.broadcasted_iota(jnp.int32, (rows, cap), 1).astype(F32)
+    for by in range(1, n_ep):
+        other = (ep + by) % n_ep
+        remote(
+            res.at[other], ret.at[other], ret_sem.at[0, other], ret_sem.at[1, other], {"ep": other}
+        ).wait_recv()
+    total = jnp.zeros((rows, ret.shape[2]), F32)
+    for e in range(n_ep):
+        pick = jnp.where(seat == key[:, e : e + 1], 1.0, 0.0).astype(BF16)
+        portion = jnp.where(one == e, part_one, 0.0) + jnp.where(two == e, part_two, 0.0)
+        total = total + portion * jnp.dot(pick, ret[e], preferred_element_type=F32)
+    out_ref[...] = total.astype(BF16)
+
+    for by in range(1, n_ep):
+        route_copy(by).wait_send()
+
+    @pl.when(z + 1 < nz)
+    def _():
+        z_copy(z, 1).wait_send()
+
+    @pl.when(z > 0)
+    def _():
+        z_copy(z, 0).wait_send()
+
+    own_copy().wait_send()
+
+    def drain(q, carry):
+        for kind in range(4):
+            h_copy(q, kind).wait_send()
+
+        @pl.when(q != z)
+        def _():
+            for kind in range(4):
+                t_copy(q, kind).wait_send()
+                sib_copy(q, kind).wait_send()
+
+        @pl.when((q < z) & (z + 1 < nz))
+        def _():
+            z_copy(q, 1).wait_send()
+
+        @pl.when((q > z) & (z > 0))
+        def _():
+            z_copy(q, 0).wait_send()
+
+        for cc in range(2):
+
+            @pl.when((q != z) | (c != cc))
+            def _():
+                ret_copy(q, cc).wait_send()
+
+        return carry
+
+    lax.fori_loop(0, nz, drain, 0)
+
+
+def moe_fused(moe_in, moe_gain, routes, route_weight, expert_gate, expert_up, expert_down):
+    n_ep = lax.axis_size("ep")
+    nz = n_ep // 2
+    rows, features = moe_in.shape
+    share = features // 4
+    ff_dev, out_dev = expert_gate.shape[2], expert_down.shape[2]
+    cap = 2 * rows * routes.shape[1] // n_ep
+    vmem = pl.BlockSpec(memory_space=pltpu.VMEM)
+    anywhere = pl.BlockSpec(memory_space=pl.ANY)
+    dma = pltpu.SemaphoreType.DMA
+    flops = 2 * n_ep * cap * features * (2 * ff_dev + out_dev)
+    return pl.pallas_call(
+        functools.partial(moe_kernel, cap),
+        out_shape=jax.ShapeDtypeStruct((rows, out_dev), BF16),
+        in_specs=[anywhere, vmem, vmem, vmem, vmem, anywhere, anywhere, anywhere],
+        out_specs=vmem,
+        scratch_shapes=[
+            pltpu.VMEM((2, nz, 4, rows, share), BF16),
+            pltpu.VMEM((nz, 4, 2 * cap, ff_dev), BF16),
+            pltpu.VMEM((2 * cap, features), BF16),
+            pltpu.VMEM((n_ep, cap, out_dev), BF16),
+            pltpu.VMEM((n_ep, cap, out_dev), BF16),
+            pltpu.VMEM((n_ep, 2, rows), jnp.int32),
+            pltpu.VMEM(expert_gate.shape[1:], BF16),
+            pltpu.VMEM(expert_up.shape[1:], BF16),
+            pltpu.VMEM(expert_down.shape[1:], BF16),
+            dma((7,)),
+            dma((2, n_ep)),
+            dma((2, nz)),
+            dma((nz,)),
+            dma((2, 4, nz)),
+            dma((2, 4, nz)),
+            dma((2,)),
+            dma((2, 4, nz)),
+            dma((2, n_ep)),
+        ],
+        compiler_params=pltpu.CompilerParams(
+            collective_id=0, has_side_effects=True, vmem_limit_bytes=48 * 1024 * 1024
+        ),
+        cost_estimate=pl.CostEstimate(flops=flops, bytes_accessed=8 << 20, transcendentals=0),
+        name="moe",
+    )(
+        moe_in,
+        moe_gain[None, :],
+        routes.T,
+        routes,
+        route_weight,
+        expert_gate,
+        expert_up,
+        expert_down,
+    )
 
 
 def from_behind(value, axis, by):
@@ -38,6 +458,61 @@
 
 def link(earlier, later):
     return (earlier[0] * later[0], later[0] * earlier[1] + later[1])
+
+
+def fits_fused(moe_in):
+    gathered = lax.axis_size("ep") * moe_in.size * moe_in.dtype.itemsize
+    return lax.axis_size("tp") == 4 and gathered <= (16 << 20)
+
+
+def moe_staged(moe_in, moe_gain, routes, route_weight, expert_gate, expert_up, expert_down):
+    moe_rows = norm_rows(moe_in, moe_gain)
+    token_count = moe_rows.shape[0]
+    feature_count = moe_rows.shape[1]
+    choose_count = routes.shape[1]
+    expert_count = lax.axis_size("ep")
+    capacity = 2 * token_count * choose_count // expert_count
+    slot_total = expert_count * capacity
+    expert_ids = routes.reshape(-1)
+    onehot = (expert_ids[:, None] == jnp.arange(expert_count, dtype=jnp.int32)[None, :]).astype(
+        jnp.int32
+    )
+    slot_rank = jnp.sum(jnp.cumsum(onehot, axis=0) * onehot, axis=1) - 1
+    slot_index = expert_ids * capacity + slot_rank
+    token_index = jnp.repeat(jnp.arange(token_count, dtype=jnp.int32), choose_count)
+    slot_owner = jnp.full((slot_total,), token_count, jnp.int32).at[slot_index].set(token_index)
+    padded_rows = jnp.concatenate([moe_rows, jnp.zeros((1, feature_count), jnp.bfloat16)], axis=0)
+    outgoing = padded_rows[slot_owner].reshape(expert_count, capacity, feature_count)
+    column_width = feature_count // lax.axis_size("tp")
+    own_columns = lax.dynamic_slice_in_dim(
+        outgoing, lax.axis_index("tp") * column_width, column_width, 2
+    )
+    incoming = lax.all_to_all(own_columns, "ep", split_axis=0, concat_axis=0, tiled=True)
+    piece = lax.all_gather(incoming, "tp", axis=2, tiled=True)
+    flat_rows = piece.reshape(slot_total, piece.shape[2])
+    gate_rows = expert_gate[0]
+    up_rows = expert_up[0]
+    gate_proj = jnp.dot(flat_rows, gate_rows, preferred_element_type=jnp.float32)
+    up_proj = jnp.dot(flat_rows, up_rows, preferred_element_type=jnp.float32)
+    hidden = (jax.nn.silu(gate_proj) * up_proj).astype(jnp.bfloat16)
+    down_rows = expert_down[0]
+    columns = jnp.dot(
+        lax.all_gather(hidden, "tp", axis=1, tiled=True),
+        down_rows,
+        preferred_element_type=jnp.float32,
+    )
+    results = columns.astype(jnp.bfloat16).reshape(expert_count, capacity, expert_down.shape[2])
+    returned = lax.all_to_all(results, "ep", split_axis=0, concat_axis=0, tiled=True).reshape(
+        slot_total, expert_down.shape[2]
+    )
+    picked = (
+        returned[slot_index]
+        .astype(jnp.float32)
+        .reshape(token_count, choose_count, expert_down.shape[2])
+    )
+    route_share = route_weight / jnp.sum(route_weight, axis=1, keepdims=True)
+    moe_out = jnp.sum(route_share[:, :, None] * picked, axis=1).astype(jnp.bfloat16)
+    return moe_out
 
 
 def local(
@@ -92,52 +567,8 @@
     carried = entering((through[row_count - 1], local_state[row_count - 1]), "ep", link, identity)
     lru_state = local_state + through * carried[1][None, :]
     mixer_out = (lru_state * jax.nn.gelu(y_branch.astype(jnp.float32))).astype(jnp.bfloat16)
-    moe_rows = norm_rows(moe_in, moe_gain)
-    token_count = moe_rows.shape[0]
-    feature_count = moe_rows.shape[1]
-    choose_count = routes.shape[1]
-    expert_count = lax.axis_size("ep")
-    capacity = 2 * token_count * choose_count // expert_count
-    slot_total = expert_count * capacity
-    expert_ids = routes.reshape(-1)
-    onehot = (expert_ids[:, None] == jnp.arange(expert_count, dtype=jnp.int32)[None, :]).astype(
-        jnp.int32
-    )
-    slot_rank = jnp.sum(jnp.cumsum(onehot, axis=0) * onehot, axis=1) - 1
-    slot_index = expert_ids * capacity + slot_rank
-    token_index = jnp.repeat(jnp.arange(token_count, dtype=jnp.int32), choose_count)
-    slot_owner = jnp.full((slot_total,), token_count, jnp.int32).at[slot_index].set(token_index)
-    padded_rows = jnp.concatenate([moe_rows, jnp.zeros((1, feature_count), jnp.bfloat16)], axis=0)
-    outgoing = padded_rows[slot_owner].reshape(expert_count, capacity, feature_count)
-    column_width = feature_count // lax.axis_size("tp")
-    own_columns = lax.dynamic_slice_in_dim(
-        outgoing, lax.axis_index("tp") * column_width, column_width, 2
-    )
-    incoming = lax.all_to_all(own_columns, "ep", split_axis=0, concat_axis=0, tiled=True)
-    piece = lax.all_gather(incoming, "tp", axis=2, tiled=True)
-    flat_rows = piece.reshape(slot_total, piece.shape[2])
-    gate_rows = expert_gate[0]
-    up_rows = expert_up[0]
-    gate_proj = jnp.dot(flat_rows, gate_rows, preferred_element_type=jnp.float32)
-    up_proj = jnp.dot(flat_rows, up_rows, preferred_element_type=jnp.float32)
-    hidden = (jax.nn.silu(gate_proj) * up_proj).astype(jnp.bfloat16)
-    down_rows = expert_down[0]
-    columns = jnp.dot(
-        lax.all_gather(hidden, "tp", axis=1, tiled=True),
-        down_rows,
-        preferred_element_type=jnp.float32,
-    )
-    results = columns.astype(jnp.bfloat16).reshape(expert_count, capacity, expert_down.shape[2])
-    returned = lax.all_to_all(results, "ep", split_axis=0, concat_axis=0, tiled=True).reshape(
-        slot_total, expert_down.shape[2]
-    )
-    picked = (
-        returned[slot_index]
-        .astype(jnp.float32)
-        .reshape(token_count, choose_count, expert_down.shape[2])
-    )
-    route_share = route_weight / jnp.sum(route_weight, axis=1, keepdims=True)
-    moe_out = jnp.sum(route_share[:, :, None] * picked, axis=1).astype(jnp.bfloat16)
+    moe_args = (moe_in, moe_gain, routes, route_weight, expert_gate, expert_up, expert_down)
+    moe_out = (moe_fused if fits_fused(moe_in) else moe_staged)(*moe_args)
     return (mixer_out, moe_out)
 
 

time: 286 us -> 178 us (0.62)
  Pallas kernels: 0 us -> 98.4 us
  waiting for transfers between devices: 63 us -> 0.01 us
  local copies, waits for them, and re-layouts: 86.2 us -> 27.8 us
  blocking collectives: 58.2 us -> 24.4 us
  other arithmetic: 32.3 us -> 13.4 us
  matrix products: 21.7 us -> 6.48 us
  between operations: 14.8 us -> 1.45 us
    pallas_call x0 -> x1, Pallas kernels: none -> 98.4 us  [moe_fused(): pl.pallas_call(functools.partial(moe_kernel, cap), out_shape=jax.ShapeDty...]
    slice x52, local copies, waits for them, and re-layouts: 60.4 us -> 8.79 us  [local(): lax.associative_scan(link, (jnp.exp(log_decay), lru_drive), axis=0)]
    all_gather x2 -> x0, waiting for transfers between devices: 42 us -> none  [the longest x1 42 us: local(): piece = lax.all_gather(incoming, 'tp', axis=2, tiled=True)]
    all_to_all x1 -> x0, blocking collectives: 31.9 us -> none  [local(): lax.all_to_all(own_columns, 'ep', split_axis=0, concat_axis=0, tiled=True)]
    all_to_all x1 -> x0, waiting for transfers between devices: 20.9 us -> none  [local(): lax.all_to_all(results, 'ep', split_axis=0, concat_axis=0, tiled=True)]
    dot_general x3 -> x0, matrix products: 14.6 us -> none  [the longest x1 6.22 us: local(): jnp.dot(lax.all_gather(hidden, 'tp', axis=1, tiled=True), down_rows, pref...]
    add x13, other arithmetic: 14.6 us -> 3.22 us  [link(): return (earlier[0] * later[0], later[0] * earlier[1] + later[1])]
    gather x2 -> x0, local copies, waits for them, and re-layouts: 8.6 us -> none  [the longest x1 5.98 us: local(): padded_rows[slot_owner].reshape(expert_count, capacity, feature_count)]
  transfers between devices with their start and end apart: 4 -> 1, of which waited for: 2 -> 0; matrix products, arithmetic and copies ran while one was open for 36% -> 0% of each run, Pallas kernels for 0% -> 56%
where the time goes in v1:
time: 178 us; the launch traced here: 177 us
  Pallas kernels  98.4 us (55%)
  local copies, waits for them, and re-layouts  27.8 us (16%)
  blocking collectives  24.4 us (14%)
  other arithmetic  13.4 us (8%)
  matrix products  6.48 us (4%)
  starting transfers between devices  4.58 us (3%)
    pallas_call x1, Pallas kernels, moe_fused(): pl.pallas_call(functools.partial(moe_kernel, cap), out_shape=jax.ShapeDty...  98.4 us
    all_gather x2, blocking collectives, entering(): everything = jax.tree.map(lambda part: lax.all_gather(part, axis), value)  24.4 us
    pad x28, local copies, waits for them, and re-layouts, local(): lax.associative_scan(link, (jnp.exp(log_decay), lru_drive), axis=0)  10.9 us
    slice x52, local copies, waits for them, and re-layouts, local(): lax.associative_scan(link, (jnp.exp(log_decay), lru_drive), axis=0)  8.79 us
    unnamed x39, local copies, waits for them, and re-layouts  5.99 us
    ppermute x1, starting transfers between devices, from_behind(): return lax.ppermute(value, axis, pairs)  4.58 us
    dot_general x1, matrix products, local(): jnp.dot(mixer_rows, w_in_y, preferred_element_type=jnp.float32)  3.77 us
  transfers between devices with their start and end apart: 1, of which 0 were waited for; matrix products, arithmetic and copies ran while one was open for 0% of the time, Pallas kernels for 56%

profile of v1, /device:TPU:1, one launch (start us, length us, event | category | flops | bytes accessed | tf_op | source)
XLA Modules:
  0.0 176.7 jit_solution(3733000463440425322)
XLA Ops:
  0.6 1.7 fusion
  2.6 2.0 %convolution_convert_fusion.1 = bf16[256,512]{1,0:T(8,128)(2,1)S(1)} fusion(bf16[2048,512]{1,0:T(8,128)(2,1)S(1)} %copy-done, bf16[256,2048]{1,0:T(8,128)(2,1)} %param.18, f32[2048]{0:T(1024)} %param.19, f32[256]{0:T(256)S(1)} %add_rsqrt_fusion), kind=kOutput, calls=%fused_computation.17 | convolution fusion | flops 539099136 | bytes 3417088 | tf_op jit(solution)/shard_map/dot_general | solution.py:542
  4.6 4.6 %collective-permute-start = (bf16[3,512]{1,0:T(4,128)(2,1)S(1)}, bf16[3,512]{1,0:T(4,128)(2,1)S(1)}, u32[]{:S(2)}, u32[]{:S(2)}) collective-permute-start(bf16[3,512]{1,0:T(4,128)(2,1)S(1)} %slice.344), channel_id=1, source_target_pairs={{0,4},{4,8},{8,12},{12,16},{16,20},{20,24},{24,28},{1,5},{5,9},{9,... | collective-permute-start | bytes 9224 | tf_op jit(solution)/shard_map/ppermute | solution.py:433
  9.6 1.6 copy-done.2
  11.1 1.6 copy-done.3
  12.7 1.2 copy-done.4
  14.0 98.4 %moe.1 = bf16[256,512]{1,0:T(8,128)(2,1)S(1)} custom-call(bf16[256,2048]{1,0:T(8,128)(2,1)S(1)} %copy-done.4, f32[1,2048]{1,0:T(1,128)S(1)} %bitcast.45, s32[2,256]{1,0:T(2,128)S(1)} %bitcast.44, s32[256,2]{1,0:T(8,128)S(1)} %copy.32.rt_col, f32[256,2]{1,0:T(8,128)S(1)} %copy.33.rw_col, bf16[1,2048,512]{2,1,0:T(8,128)(2,1)S(1)} %copy-done.2, ...), custom_call_target="tpu_custom_call" | custom-call | flops 6442450944 | bytes 8388608 | tf_op jit(solution)/shard_map/moe/pallas_call | solution.py:388
  113.1 1.0 copy.37
  114.5 1.0 copy.36
  115.5 1.9 %convert_multiply_fusion.2 = (f32[256,512]{1,0:T(8,128)S(1)}, f32[256,512]{1,0:T(8,128)S(1)}) fusion(bf16[256,512]{1,0:T(8,128)(2,1)} %copy-done.6, f32[256,512]{1,0:T(8,128)} %copy.37, f32[256,512]{1,0:T(8,128)} %param.26, f32[256,512]{1,0:T(8,128)} %copy.36, f32[512]{0:T(512)S(1)} %fusion.38), kind=kLoop, calls=%fused_computation.29 | loop fusion | flops 917504 | bytes 2885632 | tf_op jit(solution)/shard_map/mul | solution.py:563
  117.3 1.4 slice.326
  118.8 1.4 slice.272
  120.1 1.4 slice.271
  122.1 1.4 slice.269
  123.5 1.1 multiply_add_fusion.1
  131.2 1.9 %fusion.25 = (f32[127,512]{1,0:T(8,128)}, f32[127,512]{1,0:T(8,128)S(1)}) fusion(f32[127,512]{1,0:T(8,128)} %slice.326, f32[127,512]{1,0:T(8,128)} %slice.269, f32[128,512]{1,0:T(8,128)S(1)} %pad.111, f32[128,512]{1,0:T(8,128)S(1)} %pad.110, f32[128,512]{1,0:T(8,128)S(1)} %pad.127, f32[128,512]{1,0:T(8,128)S(1)} %pad.126), kind=kLoop, calls=%fused_computation.40 | loop fusion | flops 325120 | bytes 2080768 | tf_op jit(solution)/shard_map/add | solution.py:460
  133.8 2.6 %pad.128 = f32[256,512]{1,0:T(8,128)} pad(f32[128,512]{1,0:T(8,128)} %pad_maximum_fusion.2, f32[]{:T(128)} %constant.41.clone.1), padding=0_1_1x0_0_0 | pad | bytes 786436 | tf_op jit(solution)/shard_map/pad | solution.py:565
  136.4 1.7 pad_maximum_fusion.1
  138.1 2.6 %pad.112 = f32[256,512]{1,0:T(8,128)} pad(f32[128,512]{1,0:T(8,128)} %pad_maximum_fusion.1, f32[]{:T(128)} %constant.41.clone.1), padding=0_1_1x0_0_0 | pad | bytes 786436 | tf_op jit(solution)/shard_map/pad | solution.py:565
  140.7 2.6 %pad.113 = f32[256,512]{1,0:T(8,128)} pad(f32[128,512]{1,0:T(8,128)} %add.267, f32[]{:T(128)} %constant.41.clone.1), padding=1_0_1x0_0_0 | pad | bytes 786436 | tf_op jit(solution)/shard_map/pad | solution.py:565
  144.1 11.6 %all-gather.1 = f32[8,1,512]{2,1,0:T(1,128)S(1)} all-gather(f32[1,1,512]{2,1,0:T(1,128)S(1)} %add_bitcast_fusion), channel_id=1, replica_groups=mesh['ep'=8,'tp'=4] {'ep'}, dimensions={0}, use_global_device_ids=true | all-gather | bytes 18432 | tf_op jit(solution)/shard_map/all_gather | solution.py:438
  155.7 2.6 %pad.129 = f32[256,512]{1,0:T(8,128)} pad(f32[128,512]{1,0:T(8,128)} %add.276, f32[]{:T(128)} %constant.41.clone.1), padding=1_0_1x0_0_0 | pad | bytes 786436 | tf_op jit(solution)/shard_map/pad | solution.py:565
  159.0 12.8 %all-gather = f32[8,1,512]{2,1,0:T(1,128)S(1)} all-gather(f32[1,1,512]{2,1,0:T(1,128)S(1)} %add_bitcast_fusion.1), channel_id=1, replica_groups=mesh['ep'=8,'tp'=4] {'ep'}, dimensions={0}, use_global_device_ids=true | all-gather | bytes 18432 | tf_op jit(solution)/shard_map/all_gather | solution.py:438
  172.3 3.8 %fusion.18 = bf16[256,512]{1,0:T(8,128)(2,1)} fusion(bf16[2048,512]{1,0:T(8,128)(2,1)} %param.21, f32[256,512]{1,0:T(8,128)} %pad.128, f32[256,512]{1,0:T(8,128)} %pad.129, f32[256,512]{1,0:T(8,128)} %pad.112, f32[256,512]{1,0:T(8,128)} %pad.113, bf16[256,2048]{1,0:T(8,128)(2,1)S(1)} %copy-done.7, f32[2048]{0:T(1024)S(1)} %copy-done.16, ...), kind=kOutput, calls=%fused_computation.28 | convolution fusion | flops 541065216 | bytes 5516288 | tf_op jit(solution)/shard_map/dot_general | solution.py:543
  (174 shorter events, 11.7 us)
Async XLA Ops:
  0.6 1.9 %copy-start = (bf16[2048,512]{1,0:T(8,128)(2,1)S(1)}, bf16[2048,512]{1,0:T(8,128)(2,1)}, u32[]{:S(2)}) copy-start(bf16[2048,512]{1,0:T(8,128)(2,1)} %param.20) | copy-start | bytes 6291460
  2.5 2.1 %copy-start.12 = (f32[256]{0:T(256)}, f32[256]{0:T(256)S(1)}, u32[]{:S(2)}) copy-start(f32[256]{0:T(256)S(1)} %add_rsqrt_fusion) | copy-start | bytes 3076
  2.5 6.7 %copy-start.9 = (f32[4,512]{1,0:T(4,128)S(1)}, f32[4,512]{1,0:T(4,128)}, u32[]{:S(2)}) copy-start(f32[4,512]{1,0:T(4,128)} %param.22) | copy-start | bytes 24580
  2.5 6.7 %copy-start.10 = (f32[256,2]{0,1:T(2,128)S(1)}, f32[256,2]{0,1:T(2,128)}, u32[]{:S(2)}) copy-start(f32[256,2]{0,1:T(2,128)} %param.30) | copy-start | bytes 6148
  2.5 6.8 %copy-start.1 = (s32[256,2]{0,1:T(2,128)S(1)}, s32[256,2]{0,1:T(2,128)}, u32[]{:S(2)}) copy-start(s32[256,2]{0,1:T(2,128)} %param.29) | copy-start | bytes 6148
  2.6 7.0 %copy-start.5 = (f32[2048]{0:T(1024)S(1)}, f32[2048]{0:T(1024)}, u32[]{:S(2)}) copy-start(f32[2048]{0:T(1024)} %param.28) | copy-start | bytes 24580
  4.6 107.8 %collective-permute-start = (bf16[3,512]{1,0:T(4,128)(2,1)S(1)}, bf16[3,512]{1,0:T(4,128)(2,1)S(1)}, u32[]{:S(2)}, u32[]{:S(2)}) collective-permute-start(bf16[3,512]{1,0:T(4,128)(2,1)S(1)} %slice.344), channel_id=1, source_target_pairs={{0,4},{4,8},{8,12},{12,16},{16,20},{20,24},{24,28},{1,5},{5,9},{9,... | collective-permute-start | bytes 9224 | tf_op jit(solution)/shard_map/ppermute | solution.py:433
  9.5 1.6 copy-start.2
  11.1 1.6 copy-start.3
  12.7 1.2 copy-start.4
  14.0 98.4 %copy-start.11 = (f32[512]{0:T(512)S(1)}, f32[512]{0:T(512)}, u32[]{:S(2)}) copy-start(f32[512]{0:T(512)} %param.25) | copy-start | bytes 6148
  14.0 98.8 %copy-start.14 = (bf16[4,128,128]{2,1,0:T(8,128)(2,1)S(1)}, bf16[4,128,128]{2,1,0:T(8,128)(2,1)}, u32[]{:S(2)}) copy-start(bf16[4,128,128]{2,1,0:T(8,128)(2,1)} %param.24) | copy-start | bytes 393220
  112.4 1.7 copy-start.15
  112.7 1.7 copy-start.6
  127.9 0.9 copy-start.8
  133.8 38.4 %copy-start.7 = (bf16[256,2048]{1,0:T(8,128)(2,1)S(1)}, bf16[256,2048]{1,0:T(8,128)(2,1)}, u32[]{:S(2)}) copy-start(bf16[256,2048]{1,0:T(8,128)(2,1)} %param.18) | copy-start | bytes 3145732
  133.8 38.4 %copy-start.13 = (f32[256]{0:T(256)S(1)}, f32[256]{0:T(256)}, u32[]{:S(2)}) copy-start(f32[256]{0:T(256)} %copy-done.12) | copy-start | bytes 3076
  133.8 38.5 %copy-start.16 = (f32[2048]{0:T(1024)S(1)}, f32[2048]{0:T(1024)}, u32[]{:S(2)}) copy-start(f32[2048]{0:T(1024)} %param.19) | copy-start | bytes 24580

commit v2 on v1

--- a/solution.py
+++ b/solution.py
@@ -18,8 +18,25 @@
     return [sorted(range(count), key=lambda q: (abs(q - z), -q)) for z in range(count)]
 
 
-def moe_kernel(
+def one_minus_exp(value):
+    series = jnp.full_like(value, 1.0 / 9.0)
+    for k in range(8, 1, -1):
+        series = (1.0 + value * series) * (1.0 / k)
+    series = 1.0 + value * series
+    return jnp.where(value > -0.5, -value * series, 1.0 - jnp.exp(value))
+
+
+def both_kernel(
     cap,
+    mix_hbm,
+    wx_hbm,
+    wy_hbm,
+    ga_hbm,
+    gx_hbm,
+    shift_hbm,
+    mix_gain_ref,
+    taps_ref,
+    soft_ref,
     moe_hbm,
     gain_ref,
     rt_row,
@@ -28,6 +45,7 @@
     gate_hbm,
     up_hbm,
     down_hbm,
+    mix_ref,
     out_ref,
     tok,
     hid,
@@ -47,6 +65,19 @@
     own_sem,
     h_sem,
     ret_sem,
+    mixv,
+    wx,
+    wy,
+    gaw,
+    gxw,
+    shiftv,
+    xb,
+    yb,
+    av,
+    bv,
+    ends,
+    halo_sem,
+    ends_sem,
 ):
     n_ep = lax.axis_size("ep")
     nz = n_ep // 2
@@ -87,7 +118,13 @@
     ] + [
         pltpu.make_async_copy(gate_hbm.at[0], gw, load_sem.at[4]),
         pltpu.make_async_copy(up_hbm.at[0], uw, load_sem.at[5]),
-        pltpu.make_async_copy(down_hbm.at[0], dw, load_sem.at[6]),
+        pltpu.make_async_copy(mix_hbm, mixv, load_sem.at[6]),
+        pltpu.make_async_copy(wx_hbm, wx, load_sem.at[7]),
+        pltpu.make_async_copy(wy_hbm, wy, load_sem.at[8]),
+        pltpu.make_async_copy(ga_hbm, gaw, load_sem.at[9]),
+        pltpu.make_async_copy(gx_hbm, gxw, load_sem.at[10]),
+        pltpu.make_async_copy(shift_hbm, shiftv, load_sem.at[11]),
+        pltpu.make_async_copy(down_hbm.at[0], dw, load_sem.at[12]),
     ]
     for copy in loads:
         copy.start()
@@ -241,6 +278,127 @@
             def _():
                 ret[ep] = res[q * 2 + cc]
 
+    pad = xb.shape[0] - rows
+
+    def halo_copy():
+        return remote(
+            xb.at[pl.ds(rows, pad)],
+            xb.at[pl.ds(0, pad)],
+            halo_sem.at[0],
+            halo_sem.at[1],
+            {"ep": ep + 1},
+        )
+
+    def ends_copy(by):
+        return remote(
+            ends.at[ep],
+            ends.at[ep],
+            ends_sem.at[0, by],
+            ends_sem.at[1, ep],
+            {"ep": (ep + by) % n_ep},
+        )
+
+    def project():
+        for k in range(6, 9):
+            loads[k].wait()
+        strip = 64
+
+        @pl.loop(0, rows // strip)
+        def _(i):
+            at = pl.ds(pl.multiple_of(i * strip, strip), strip)
+            wide = mixv[at, :].astype(F32)
+            scale = lax.rsqrt(jnp.mean(wide * wide, axis=-1, keepdims=True) + epsilon)
+            xs[at, :] = (wide * scale * mix_gain_ref[...]).astype(BF16)
+
+        tile = 256
+
+        @pl.loop(0, wx.shape[1] // tile)
+        def _(j):
+            cols = pl.ds(pl.multiple_of(j * tile, tile), tile)
+            xb[pl.ds(pad, rows), cols] = jnp.dot(
+                xs[...], wx[:, cols], preferred_element_type=F32
+            ).astype(BF16)
+            yb[:, cols] = jnp.dot(xs[...], wy[:, cols], preferred_element_type=F32).astype(BF16)
+
+        @pl.when(ep + 1 < n_ep)
+        def _():
+            halo_copy().start()
+
+        @pl.when(ep == 0)
+        def _():
+            xb[pl.ds(0, pad), :] = jnp.zeros((pad, xb.shape[1]), BF16)
+
+    def recur():
+        for k in range(9, 12):
+            loads[k].wait()
+
+        @pl.when(ep > 0)
+        def _():
+            halo_copy().wait_recv()
+
+        taps = taps_ref.shape[0]
+        size = gaw.shape[1]
+        for h in range(gaw.shape[0]):
+            cols = pl.ds(h * size, size)
+            wide = xb[:, cols].astype(F32)
+            conv = jnp.zeros((rows, size), F32)
+            for k in range(taps):
+                first_row = pad - (taps - 1) + k
+                conv = conv + taps_ref[k : k + 1, cols] * wide[first_row : first_row + rows]
+            x_conv = conv.astype(BF16)
+            gate_a = jnp.dot(x_conv, gaw[h], preferred_element_type=F32)
+            gate_x = jnp.dot(x_conv, gxw[h], preferred_element_type=F32)
+            log_decay = (
+                -lru_scale * jax.nn.sigmoid(gate_a) * soft_ref[:, cols] + shiftv[:, cols]
+            )
+            av[:, cols] = jnp.exp(log_decay)
+            bv[:, cols] = (
+                jnp.sqrt(one_minus_exp(2.0 * log_decay))
+                * jax.nn.sigmoid(gate_x)
+                * x_conv.astype(F32)
+            )
+        width = av.shape[1]
+        row = lax.broadcasted_iota(jnp.int32, (8, width), 0)
+
+        def group(i, carry):
+            at = pl.ds(pl.multiple_of(i * 8, 8), 8)
+            a, b = av[at, :], bv[at, :]
+            for by in (1, 2, 4):
+                a_past, b_past = pltpu.roll(a, by, 0), pltpu.roll(b, by, 0)
+                b = jnp.where(row >= by, a * b_past + b, b)
+                a = jnp.where(row >= by, a * a_past, a)
+            b = a * carry[1] + b
+            a = a * carry[0]
+            av[at, :] = a
+            bv[at, :] = b
+            return (a[7:8], b[7:8])
+
+        through, state = lax.fori_loop(
+            0, rows // 8, group, (jnp.ones((1, width), F32), jnp.zeros((1, width), F32))
+        )
+        ends[ep, 0:1] = through
+        ends[ep, 1:2] = state
+        for by in range(1, n_ep):
+            ends_copy(by).start()
+
+    def finish():
+        carried = jnp.zeros((1, av.shape[1]), F32)
+        for by in range(1, n_ep):
+            other = (ep + by) % n_ep
+            remote(
+                ends.at[other], ends.at[other], ends_sem.at[0, 0], ends_sem.at[1, other], {"ep": other}
+            ).wait_recv()
+        for k in range(n_ep):
+            entered = ends[k, 0:1] * carried + ends[k, 1:2]
+            carried = jnp.where(k < ep, entered, carried)
+        strip = 32
+
+        @pl.loop(0, rows // strip)
+        def _(i):
+            at = pl.ds(pl.multiple_of(i * strip, strip), strip)
+            state = bv[at, :] + av[at, :] * carried
+            mix_ref[at, :] = (state * jax.nn.gelu(yb[at, :].astype(F32))).astype(BF16)
+
     for k in range(4):
         loads[k].wait()
 
@@ -253,7 +411,7 @@
         z_copy(z, 0).start()
 
     own_copy().start()
-    for k in range(4, 7):
+    for k in range(4, 6):
         loads[k].wait()
     for by in range(1, n_ep):
         other = (ep + by) % n_ep
@@ -268,14 +426,24 @@
     z_copy(first, 1).wait_recv()
     spread(first)
 
+    def pass_hidden(q):
+        h_copy(q, 0).wait_recv()
+        h_copy(q, 3).start()
+        h_copy(q, 1).wait_recv()
+        h_copy(q, 2).start()
+
+    project()
+    pass_hidden(z)
+    loads[12].wait()
+
     def step(s, carry):
         q = block_at(s)
         nxt = block_at(s + 1)
         far = block_at(s + 2)
-        h_copy(q, 0).wait_recv()
-        h_copy(q, 3).start()
-        h_copy(q, 1).wait_recv()
-        h_copy(q, 2).start()
+
+        @pl.when(s + 1 == nz)
+        def _():
+            pass_hidden(q)
 
         @pl.when(s + 1 < nz)
         def _():
@@ -291,6 +459,10 @@
                 z_copy(far, 1).wait_recv()
                 spread(far)
 
+            @pl.when(s > 0)
+            def _():
+                pass_hidden(q)
+
             t_copy(nxt, 2).wait_recv()
             t_copy(nxt, 3).wait_recv()
             sib_copy(nxt, dg).start()
@@ -301,6 +473,15 @@
         h_copy(q, 2).wait_recv()
         h_copy(q, 3).wait_recv()
         expert_out(q)
+
+        @pl.when(s == 0)
+        def _():
+            recur()
+
+        @pl.when(s == 1)
+        def _():
+            finish()
+
         return carry
 
     lax.fori_loop(0, nz, step, 0)
@@ -345,6 +526,13 @@
 
     own_copy().wait_send()
 
+    @pl.when(ep + 1 < n_ep)
+    def _():
+        halo_copy().wait_send()
+
+    for by in range(1, n_ep):
+        ends_copy(by).wait_send()
+
     def drain(q, carry):
         for kind in range(4):
             h_copy(q, kind).wait_send()
@@ -374,22 +562,43 @@
     lax.fori_loop(0, nz, drain, 0)
 
 
-def moe_fused(moe_in, moe_gain, routes, route_weight, expert_gate, expert_up, expert_down):
+def both_fused(
+    mix_in,
+    mix_gain,
+    w_in_x,
+    w_in_y,
+    conv_taps,
+    recur_gate_w,
+    input_gate_w,
+    decay_logit,
+    decay_shift,
+    moe_in,
+    moe_gain,
+    routes,
+    route_weight,
+    expert_gate,
+    expert_up,
+    expert_down,
+):
     n_ep = lax.axis_size("ep")
     nz = n_ep // 2
     rows, features = moe_in.shape
     share = features // 4
     ff_dev, out_dev = expert_gate.shape[2], expert_down.shape[2]
+    width = w_in_x.shape[1]
     cap = 2 * rows * routes.shape[1] // n_ep
     vmem = pl.BlockSpec(memory_space=pltpu.VMEM)
-    anywhere = pl.BlockSpec(memory_space=pl.ANY)
+    hbm = pl.BlockSpec(memory_space=pltpu.HBM)
     dma = pltpu.SemaphoreType.DMA
     flops = 2 * n_ep * cap * features * (2 * ff_dev + out_dev)
     return pl.pallas_call(
-        functools.partial(moe_kernel, cap),
-        out_shape=jax.ShapeDtypeStruct((rows, out_dev), BF16),
-        in_specs=[anywhere, vmem, vmem, vmem, vmem, anywhere, anywhere, anywhere],
-        out_specs=vmem,
+        functools.partial(both_kernel, cap),
+        out_shape=(
+            jax.ShapeDtypeStruct((rows, width), BF16),
+            jax.ShapeDtypeStruct((rows, out_dev), BF16),
+        ),
+        in_specs=[hbm] * 6 + [vmem] * 3 + [hbm] + [vmem] * 4 + [hbm] * 3,
+        out_specs=(vmem, vmem),
         scratch_shapes=[
             pltpu.VMEM((2, nz, 4, rows, share), BF16),
             pltpu.VMEM((nz, 4, 2 * cap, ff_dev), BF16),
@@ -400,7 +609,7 @@
             pltpu.VMEM(expert_gate.shape[1:], BF16),
             pltpu.VMEM(expert_up.shape[1:], BF16),
             pltpu.VMEM(expert_down.shape[1:], BF16),
-            dma((7,)),
+            dma((13,)),
             dma((2, n_ep)),
             dma((2, nz)),
             dma((nz,)),
@@ -409,13 +618,35 @@
             dma((2,)),
             dma((2, 4, nz)),
             dma((2, n_ep)),
+            pltpu.VMEM(mix_in.shape, BF16),
+            pltpu.VMEM(w_in_x.shape, BF16),
+            pltpu.VMEM(w_in_y.shape, BF16),
+            pltpu.VMEM(recur_gate_w.shape, BF16),
+            pltpu.VMEM(input_gate_w.shape, BF16),
+            pltpu.VMEM((rows, width), F32),
+            pltpu.VMEM((16 + rows, width), BF16),
+            pltpu.VMEM((rows, width), BF16),
+            pltpu.VMEM((rows, width), F32),
+            pltpu.VMEM((rows, width), F32),
+            pltpu.VMEM((n_ep, 2, width), F32),
+            dma((2,)),
+            dma((2, n_ep)),
         ],
         compiler_params=pltpu.CompilerParams(
-            collective_id=0, has_side_effects=True, vmem_limit_bytes=48 * 1024 * 1024
+            collective_id=0, has_side_effects=True, vmem_limit_bytes=60 * 1024 * 1024
         ),
-        cost_estimate=pl.CostEstimate(flops=flops, bytes_accessed=8 << 20, transcendentals=0),
-        name="moe",
+        cost_estimate=pl.CostEstimate(flops=flops, bytes_accessed=16 << 20, transcendentals=0),
+        name="both",
     )(
+        mix_in,
+        w_in_x,
+        w_in_y,
+        recur_gate_w,
+        input_gate_w,
+        decay_shift,
+        mix_gain[None, :],
+        conv_taps,
+        jax.nn.softplus(-decay_logit)[None, :],
         moe_in,
         moe_gain[None, :],
         routes.T,
@@ -460,9 +691,11 @@
     return (earlier[0] * later[0], later[0] * earlier[1] + later[1])
 
 
-def fits_fused(moe_in):
-    gathered = lax.axis_size("ep") * moe_in.size * moe_in.dtype.itemsize
-    return lax.axis_size("tp") == 4 and gathered <= (16 << 20)
+def fits_fused(moe_in, routes):
+    n_ep = lax.axis_size("ep")
+    gathered = n_ep * moe_in.size * moe_in.dtype.itemsize
+    even = n_ep == 4 * routes.shape[1]
+    return lax.axis_size("tp") == 4 and even and gathered <= (16 << 20)
 
 
 def moe_staged(moe_in, moe_gain, routes, route_weight, expert_gate, expert_up, expert_down):
@@ -515,7 +748,7 @@
     return moe_out
 
 
-def local(
+def staged(
     mix_in,
     mix_gain,
     w_in_x,
@@ -567,9 +800,14 @@
     carried = entering((through[row_count - 1], local_state[row_count - 1]), "ep", link, identity)
     lru_state = local_state + through * carried[1][None, :]
     mixer_out = (lru_state * jax.nn.gelu(y_branch.astype(jnp.float32))).astype(jnp.bfloat16)
-    moe_args = (moe_in, moe_gain, routes, route_weight, expert_gate, expert_up, expert_down)
-    moe_out = (moe_fused if fits_fused(moe_in) else moe_staged)(*moe_args)
+    moe_out = moe_staged(
+        moe_in, moe_gain, routes, route_weight, expert_gate, expert_up, expert_down
+    )
     return (mixer_out, moe_out)
+
+
+def local(*args):
+    return (both_fused if fits_fused(args[9], args[11]) else staged)(*args)
 
 
 def solution(mesh):

time: 178 us -> 103 us (0.58)
  blocking collectives: 24.4 us -> 0 us
  local copies, waits for them, and re-layouts: 27.8 us -> 6.29 us
  other arithmetic: 13.4 us -> 1.28 us
  matrix products: 6.48 us -> 0 us
  starting transfers between devices: 4.58 us -> 0 us
  Pallas kernels: 98.4 us -> 94.2 us
    all_gather x2 -> x0, blocking collectives: 24.4 us -> none  [entering(): everything = jax.tree.map(lambda part: lax.all_gather(part, axis), value)]
    pad x28 -> x0, local copies, waits for them, and re-layouts: 10.9 us -> none  [local(): lax.associative_scan(link, (jnp.exp(log_decay), lru_drive), axis=0)]
    slice x54 -> x0, local copies, waits for them, and re-layouts: 8.81 us -> none  [the longest x52 8.79 us: local(): lax.associative_scan(link, (jnp.exp(log_decay), lru_drive), axis=0)]
    dot_general x4 -> x0, matrix products: 6.48 us -> none  [the longest x1 3.77 us: local(): jnp.dot(mixer_rows, w_in_y, preferred_element_type=jnp.float32)]
    add x26 -> x0, other arithmetic: 4.81 us -> none  [the longest x13 3.22 us: link(): return (earlier[0] * later[0], later[0] * earlier[1] + later[1])]
    ppermute x1 -> x0, starting transfers between devices: 4.58 us -> none  [from_behind(): return lax.ppermute(value, axis, pairs)]
    pallas_call x1, Pallas kernels: 98.4 us -> 94.2 us  [both_fused(): pl.pallas_call(functools.partial(both_kernel, cap), out_shape=(jax.ShapeD...]
    concatenate x13 -> x0, other arithmetic: 3.2 us -> none  [local(): lax.associative_scan(link, (jnp.exp(log_decay), lru_drive), axis=0)]
  transfers between devices with their start and end apart: 1 -> 0, of which waited for: 0 -> 0; matrix products, arithmetic and copies ran while one was open for 0% -> 0% of each run, Pallas kernels for 56% -> 0%
where the time goes in v2:
time: 103 us; the launch traced here: 102 us
  Pallas kernels  94.2 us (91%)
  local copies, waits for them, and re-layouts  6.29 us (6%)
  other arithmetic  1.28 us (1%)
    pallas_call x1, Pallas kernels, both_fused(): pl.pallas_call(functools.partial(both_kernel, cap), out_shape=(jax.ShapeD...  94.2 us
    unnamed x4, local copies, waits for them, and re-layouts  6.29 us

profile of v2, /device:TPU:1, one launch (start us, length us, event | category | flops | bytes accessed | tf_op | source)
XLA Modules:
  0.0 102.5 jit_solution(12323853878414900454)
XLA Ops:
  0.6 1.3 %compare_select_fusion = f32[512]{0:T(512)} fusion(f32[512]{0:T(512)} %param.23), kind=kLoop, calls=%fused_computation | loop fusion | flops 3584 | bytes 4096 | tf_op jit(solution)/shard_map/jit(softplus)/select_n | solution.py:649
  1.9 1.5 %copy.19.rw_col = f32[256,2]{1,0:T(8,128)} copy(f32[256,2]{0,1:T(2,128)} %param.28) | data formatting | bytes 4096 | tf_op args[12]
  3.4 1.5 %copy.18.rt_col = s32[256,2]{1,0:T(8,128)} copy(s32[256,2]{0,1:T(2,128)} %param.27) | data formatting | bytes 4096 | tf_op args[11]
  4.9 94.2 %both.1 = (bf16[256,512]{1,0:T(8,128)(2,1)}, bf16[256,512]{1,0:T(8,128)(2,1)}) custom-call(bf16[256,2048]{1,0:T(8,128)(2,1)} %mix_hbm.1, bf16[2048,512]{1,0:T(8,128)(2,1)} %wx_hbm.1, bf16[2048,512]{1,0:T(8,128)(2,1)} %wy_hbm.1, bf16[4,128,128]{2,1,0:T(8,128)(2,1)} %ga_hbm.1, bf16[4,128,128]{2,1,0:T(8,128)(2,1)} %gx_hbm.1, f32[256,512]{1,0:T(8,128)} %shift_hbm.1, ...), custom_call_target="tpu_custom_call" | custom-call | flops 6442450944 | bytes 16777216 | tf_op jit(solution)/shard_map/both/pallas_call | solution.py:594
  99.1 1.7 %copy.22 = bf16[256,512]{1,0:T(8,128)(2,1)} copy(bf16[256,512]{1,0:T(8,128)(2,1)} %get-tuple-element.4) | data formatting | bytes 524288
  100.8 1.7 %copy.23 = bf16[256,512]{1,0:T(8,128)(2,1)} copy(bf16[256,512]{1,0:T(8,128)(2,1)} %get-tuple-element.5) | data formatting | bytes 524288

commit v3 on v2

--- a/solution.py
+++ b/solution.py
@@ -14,8 +14,7 @@
 BF16 = jnp.bfloat16
 
 
-def near_first(count):
-    return [sorted(range(count), key=lambda q: (abs(q - z), -q)) for z in range(count)]
+block_order = ((0, 2, 3, 1), (1, 2, 3, 0), (2, 1, 0, 3), (3, 1, 0, 2))
 
 
 def one_minus_exp(value):
@@ -40,8 +39,7 @@
     moe_hbm,
     gain_ref,
     rt_row,
-    rt_col,
-    rw_col,
+    rw_row,
     gate_hbm,
     up_hbm,
     down_hbm,
@@ -91,7 +89,7 @@
     pair = 2 * cap
     pair_half = pair // 2
     sibling = {"ep": z * 2 + (1 - c)}
-    table = near_first(nz)
+    table = block_order
 
     def block_at(s):
         q = jnp.int32(0)
@@ -161,14 +159,10 @@
         )
 
     def t_copy(q, kind):
-        if kind == 0:
-            part, where = tok.at[c, q, t], {"tp": xp}
-        elif kind == 1:
-            part, where = tok.at[c, q, t], {"tp": yp}
-        elif kind == 2:
-            part, where = tok.at[c, q, yp, pl.ds(half, half)], {"tp": xp}
-        else:
-            part, where = tok.at[c, q, xp, pl.ds(0, half)], {"tp": yp}
+        owner = (t, t, t, t, yp, xp)[kind]
+        start = (0, half, half, 0, half, 0)[kind]
+        part = tok.at[c, q, owner, pl.ds(start, half)]
+        where = {"tp": (xp, yp)[kind % 2]}
         return remote(part, part, t_sem.at[0, kind, q], t_sem.at[1, kind, q], where)
 
     def sib_copy(q, k):
@@ -180,14 +174,10 @@
         return remote(part, part, own_sem.at[0], own_sem.at[1], sibling)
 
     def h_copy(q, kind):
-        if kind == 0:
-            part, where = hid.at[q, t], {"tp": xp}
-        elif kind == 1:
-            part, where = hid.at[q, t], {"tp": yp}
-        elif kind == 2:
-            part, where = hid.at[q, yp, pl.ds(pair_half, pair_half)], {"tp": xp}
-        else:
-            part, where = hid.at[q, xp, pl.ds(0, pair_half)], {"tp": yp}
+        owner = (t, t, t, t, yp, xp)[kind]
+        start = (0, pair_half, pair_half, 0, pair_half, 0)[kind]
+        part = hid.at[q, owner, pl.ds(start, pair_half)]
+        where = {"tp": (xp, yp)[kind % 2]}
         return remote(part, part, h_sem.at[0, kind, q], h_sem.at[1, kind, q], where)
 
     def ret_copy(q, cc):
@@ -197,8 +187,12 @@
         )
 
     def spread(q):
-        t_copy(q, 0).start()
-        t_copy(q, 1).start()
+        for kind in range(4):
+            t_copy(q, kind).start()
+        sib_copy(q, t).start()
+
+    def arrive(q):
+        z_copy(q, 1).wait_recv()
 
         @pl.when((q < z) & (z + 1 < nz))
         def _():
@@ -207,8 +201,6 @@
         @pl.when((q > z) & (z > 0))
         def _():
             z_copy(q, 0).start()
-
-        sib_copy(q, t).start()
 
     def ranks_row(block):
         named = routes_all[block]
@@ -248,8 +240,8 @@
             u = jnp.dot(xs[...], uw[:, cols], preferred_element_type=F32)
             hid[q, t, :, cols] = (jax.nn.silu(g) * u).astype(BF16)
 
-        h_copy(q, 0).start()
-        h_copy(q, 1).start()
+        for kind in range(4):
+            h_copy(q, kind).start()
 
     def expert_out(q):
         tile = 256
@@ -328,7 +320,7 @@
         def _():
             xb[pl.ds(0, pad), :] = jnp.zeros((pad, xb.shape[1]), BF16)
 
-    def recur():
+    def drives():
         for k in range(9, 12):
             loads[k].wait()
 
@@ -357,6 +349,8 @@
                 * jax.nn.sigmoid(gate_x)
                 * x_conv.astype(F32)
             )
+
+    def recur():
         width = av.shape[1]
         row = lax.broadcasted_iota(jnp.int32, (8, width), 0)
 
@@ -423,18 +417,34 @@
     ).wait_recv()
     expert_in(z)
     first = block_at(1)
-    z_copy(first, 1).wait_recv()
+
+    @pl.when(z > 0)
+    def _():
+        arrive(z - 1)
+
+    @pl.when(z + 1 < nz)
+    def _():
+        arrive(z + 1)
+
+    @pl.when((first == z + 2) | (first == z - 2))
+    def _():
+        arrive(first)
+
     spread(first)
 
     def pass_hidden(q):
         h_copy(q, 0).wait_recv()
-        h_copy(q, 3).start()
+        h_copy(q, 5).start()
         h_copy(q, 1).wait_recv()
-        h_copy(q, 2).start()
+        h_copy(q, 4).start()
 
     project()
     pass_hidden(z)
     loads[12].wait()
+
+    @pl.when((z > 0) & (z + 1 < nz))
+    def _():
+        arrive(jnp.where(z + 2 < nz, z + 2, z - 2))
 
     def step(s, carry):
         q = block_at(s)
@@ -448,15 +458,16 @@
         @pl.when(s + 1 < nz)
         def _():
             t_copy(nxt, 0).wait_recv()
-            t_copy(nxt, 3).start()
-            sib_copy(nxt, xp).start()
+            t_copy(nxt, 5).start()
             t_copy(nxt, 1).wait_recv()
-            t_copy(nxt, 2).start()
-            sib_copy(nxt, yp).start()
+            t_copy(nxt, 4).start()
 
             @pl.when(s + 2 < nz)
             def _():
-                z_copy(far, 1).wait_recv()
+                @pl.when((far == z + 3) | (far == z - 3))
+                def _():
+                    arrive(far)
+
                 spread(far)
 
             @pl.when(s > 0)
@@ -464,21 +475,29 @@
                 pass_hidden(q)
 
             t_copy(nxt, 2).wait_recv()
+            sib_copy(nxt, xp).start()
             t_copy(nxt, 3).wait_recv()
+            sib_copy(nxt, yp).start()
+            t_copy(nxt, 4).wait_recv()
+            t_copy(nxt, 5).wait_recv()
             sib_copy(nxt, dg).start()
             for k in range(4):
                 sib_copy(nxt, k).wait_recv()
             expert_in(nxt)
 
-        h_copy(q, 2).wait_recv()
-        h_copy(q, 3).wait_recv()
+        for kind in range(2, 6):
+            h_copy(q, kind).wait_recv()
         expert_out(q)
 
         @pl.when(s == 0)
         def _():
+            drives()
+
+        @pl.when(s == 1)
+        def _():
             recur()
 
-        @pl.when(s == 1)
+        @pl.when(s == 2)
         def _():
             finish()
 
@@ -486,7 +505,16 @@
 
     lax.fori_loop(0, nz, step, 0)
 
-    one, two = rt_col[:, 0:1], rt_col[:, 1:2]
+    weights = rw_row[...]
+    columns = jnp.concatenate(
+        [
+            rt_row[...].astype(F32),
+            weights / (weights[0:1] + weights[1:2]),
+            jnp.zeros((124, rows), F32),
+        ],
+        axis=0,
+    ).T
+    one, two = columns[:, 0:1].astype(jnp.int32), columns[:, 1:2].astype(jnp.int32)
     lane = lax.broadcasted_iota(jnp.int32, (rows, 128), 1)
     mask = jnp.where((one == lane) | (two == lane), 1.0, 0.0)
     before = jnp.where(
@@ -497,9 +525,7 @@
     ).astype(BF16)
     rank = jnp.dot(before, mask.astype(BF16), preferred_element_type=F32)
     key = jnp.where(mask > 0.5, rank, -1.0)
-    total_weight = rw_col[:, 0:1] + rw_col[:, 1:2]
-    part_one = rw_col[:, 0:1] / total_weight
-    part_two = rw_col[:, 1:2] / total_weight
+    part_one, part_two = columns[:, 2:3], columns[:, 3:4]
     seat = lax.broadcasted_iota(jnp.int32, (rows, cap), 1).astype(F32)
     for by in range(1, n_ep):
         other = (ep + by) % n_ep
@@ -534,14 +560,15 @@
         ends_copy(by).wait_send()
 
     def drain(q, carry):
-        for kind in range(4):
+        for kind in range(6):
             h_copy(q, kind).wait_send()
 
         @pl.when(q != z)
         def _():
-            for kind in range(4):
+            for kind in range(6):
                 t_copy(q, kind).wait_send()
-                sib_copy(q, kind).wait_send()
+            for k in range(4):
+                sib_copy(q, k).wait_send()
 
         @pl.when((q < z) & (z + 1 < nz))
         def _():
@@ -597,7 +624,7 @@
             jax.ShapeDtypeStruct((rows, width), BF16),
             jax.ShapeDtypeStruct((rows, out_dev), BF16),
         ),
-        in_specs=[hbm] * 6 + [vmem] * 3 + [hbm] + [vmem] * 4 + [hbm] * 3,
+        in_specs=[hbm] * 6 + [vmem] * 3 + [hbm] + [vmem] * 3 + [hbm] * 3,
         out_specs=(vmem, vmem),
         scratch_shapes=[
             pltpu.VMEM((2, nz, 4, rows, share), BF16),
@@ -613,10 +640,10 @@
             dma((2, n_ep)),
             dma((2, nz)),
             dma((nz,)),
-            dma((2, 4, nz)),
+            dma((2, 6, nz)),
             dma((2, 4, nz)),
             dma((2,)),
-            dma((2, 4, nz)),
+            dma((2, 6, nz)),
             dma((2, n_ep)),
             pltpu.VMEM(mix_in.shape, BF16),
             pltpu.VMEM(w_in_x.shape, BF16),
@@ -650,8 +677,7 @@
         moe_in,
         moe_gain[None, :],
         routes.T,
-        routes,
-        route_weight,
+        route_weight.T,
         expert_gate,
         expert_up,
         expert_down,
@@ -694,7 +720,7 @@
 def fits_fused(moe_in, routes):
     n_ep = lax.axis_size("ep")
     gathered = n_ep * moe_in.size * moe_in.dtype.itemsize
-    even = n_ep == 4 * routes.shape[1]
+    even = n_ep == 4 * routes.shape[1] == 2 * len(block_order)
     return lax.axis_size("tp") == 4 and even and gathered <= (16 << 20)
 
 

time: 103 us -> 94.5 us (0.917)
  Pallas kernels: 94.2 us -> 89 us
  local copies, waits for them, and re-layouts: 6.29 us -> 3.34 us
    pallas_call x1, Pallas kernels: 94.2 us -> 89 us  [both_fused(): pl.pallas_call(functools.partial(both_kernel, cap), out_shape=(jax.ShapeD...]
    unnamed x4 -> x2, local copies, waits for them, and re-layouts: 6.29 us -> 3.34 us
where the time goes in v3:
time: 94.5 us; the launch traced here: 94.3 us
  Pallas kernels  89 us (94%)
  local copies, waits for them, and re-layouts  3.34 us (4%)
  other arithmetic  1.28 us (1%)
    pallas_call x1, Pallas kernels, both_fused(): pl.pallas_call(functools.partial(both_kernel, cap), out_shape=(jax.ShapeD...  89 us
    unnamed x2, local copies, waits for them, and re-layouts  3.34 us

profile of v3, /device:TPU:1, one launch (start us, length us, event | category | flops | bytes accessed | tf_op | source)
XLA Modules:
  0.0 94.3 jit_solution(2718100735016470244)
XLA Ops:
  0.6 1.3 %compare_select_fusion = f32[512]{0:T(512)} fusion(f32[512]{0:T(512)} %param.23), kind=kLoop, calls=%fused_computation | loop fusion | flops 3584 | bytes 4096 | tf_op jit(solution)/shard_map/jit(softplus)/select_n | solution.py:676
  1.9 89.0 %both.1 = (bf16[256,512]{1,0:T(8,128)(2,1)}, bf16[256,512]{1,0:T(8,128)(2,1)}) custom-call(bf16[256,2048]{1,0:T(8,128)(2,1)} %mix_hbm.1, bf16[2048,512]{1,0:T(8,128)(2,1)} %wx_hbm.1, bf16[2048,512]{1,0:T(8,128)(2,1)} %wy_hbm.1, bf16[4,128,128]{2,1,0:T(8,128)(2,1)} %ga_hbm.1, bf16[4,128,128]{2,1,0:T(8,128)(2,1)} %gx_hbm.1, f32[256,512]{1,0:T(8,128)} %shift_hbm.1, ...), custom_call_target="tpu_custom_call" | custom-call | flops 6442450944 | bytes 16777216 | tf_op jit(solution)/shard_map/both/pallas_call | solution.py:621
  90.9 1.7 %copy.20 = bf16[256,512]{1,0:T(8,128)(2,1)} copy(bf16[256,512]{1,0:T(8,128)(2,1)} %get-tuple-element.4) | data formatting | bytes 524288
  92.6 1.7 %copy.21 = bf16[256,512]{1,0:T(8,128)(2,1)} copy(bf16[256,512]{1,0:T(8,128)(2,1)} %get-tuple-element.5) | data formatting | bytes 524288
